TPU v7x, 32 devices: a whole 2x2x4 slice. The times are simulated.
32 devices in a mesh: grp: 2 (over x), row: 4 (over z), col: 4 (over y, core).
Axes of the slice: x: 2, y: 2, z: 4, core: 2. Of those that a mesh axis runs over, the one named last changes fastest.
Arguments:
- gate_in: bfloat16 [8, 512, 1024], P(('grp', 'row'), 'col'), parts along dimension 0, may hold values from -6 to 6
- mult_in: bfloat16 [8, 512, 1024], P(('grp', 'row'), 'col'), parts along dimension 0, may hold values from -6 to 6
- value_in: bfloat16 [8, 512, 1024], P(('grp', 'row'), 'col'), parts along dimension 0, may hold values from -6 to 6
- taps_gate: float32 [3, 1024], replicated, may hold values from -3.5 to 3.5
- taps_mult: float32 [3, 1024], replicated, may hold values from -3.5 to 3.5
- taps_value: float32 [3, 1024], replicated, may hold values from -3.5 to 3.5
- filter_first: float32 [33, 128], replicated, may hold values from -3 to 3
- filter_second: float32 [128, 128], replicated, may hold values from -1 to 1
- filter_ahead: float32 [128, 1024], replicated, may hold values from -0.5 to 0.5
- filter_behind: float32 [128, 1024], replicated, may hold values from -0.5 to 0.5
- filter_decay: float32 [1024], replicated, may hold values from 0.05 to 17.033333
- skip_gain: float32 [1024], replicated, may hold values from -5 to 5
- out_weight: bfloat16 [1024, 2048], replicated, may hold values from -0.1875 to 0.1875
Outputs:
- mixed: bfloat16 [8, 512, 2048], P(('grp', 'row'), 'col'), parts along dimension 0
There are 2 independent parts, one for each index of `grp`. A program takes and returns all parts, laid end to end along the dimension named above; an argument that names none is the same for every part. Nothing has to cross between parts.
All inputs are finite; a program needn't handle non-finite values.
Results may differ from a plain program's by a relative error of at most 0.0049.
Values may be sent and summed in bfloat16 or wider, within the bound.
A program may use at most 64 MiB of HBM per device.

v0:
```python
import math
import jax
import jax.numpy as jnp
from jax import lax
from jax.sharding import PartitionSpec as P

highest = lax.Precision.HIGHEST


def padded_2(shard, sides, width):
    for axis, dim in sides:
        size, length = (lax.axis_size(axis), shard.shape[dim])
        up = [(i, (i + 1) % size) for i in range(size - 1)]
        down = [(j, i) for i, j in up]
        last = lax.slice_in_dim(shard, length - width, length, axis=dim)
        leading = lax.slice_in_dim(shard, 0, width, axis=dim)
        before = lax.ppermute(last, axis, up)
        after = lax.ppermute(leading, axis, down)
        shard = jnp.concatenate([before, shard, after], axis=dim)
    return shard


def filter_hidden(mirror, seq_len, filter_first, filter_second):
    tau_values = mirror.astype(jnp.float32) / (seq_len - 1)
    omega_pos = 2.0 * math.pi / seq_len * mirror.astype(jnp.float32)
    band_count = (filter_first.shape[0] - 1) // 2
    band_values = jnp.linspace(0.0001, band_count - 1, band_count, dtype=jnp.float32)
    angles = omega_pos[:, None] * band_values[None, :]
    features = jnp.concatenate([tau_values[:, None], jnp.cos(angles), -jnp.sin(angles)], axis=1)
    hidden = jnp.sin(jnp.dot(features, filter_first, precision=highest))
    hidden = jnp.sin(jnp.dot(hidden, filter_second, precision=highest))
    return (hidden, tau_values)


def side_values(hidden, tau_values, side_weight, decay_rates):
    values = jnp.einsum("pf,fh->hp", hidden, side_weight, precision=highest)
    return values * jnp.exp(-decay_rates[:, None] * tau_values[None, :])


def angle_table(row_count, column_count, period):
    products = (
        lax.iota(jnp.int32, row_count)[:, None]
        * lax.iota(jnp.int32, column_count)[None, :]
        % period
    )
    angle = products.astype(jnp.float32) * (2.0 * math.pi / period)
    return (jnp.cos(angle), jnp.sin(angle))


def swap_halves(stacked, width):
    return jnp.concatenate([stacked[..., width:], stacked[..., :width]], axis=-1)


def forward(values, first_table, twist_even, twist_odd, second_block):
    channels, _, width = values.shape
    first = jnp.einsum("sfa,cab->cfsb", first_table, values, precision=highest)
    first = first.reshape(channels, first_table.shape[1], 2 * width)
    turned = first * twist_even + swap_halves(first, width) * twist_odd
    return jnp.einsum("cfk,kl->cfl", turned, second_block, precision=highest)


def inverse(spectrum, last_table, twist_even, twist_odd, second_block, span_len):
    channels, freq_rows, double_width = spectrum.shape
    width = double_width // 2
    back = jnp.einsum("cfk,kl->cfl", spectrum, second_block, precision=highest)
    turned = back * twist_even + swap_halves(back, width) * twist_odd
    turned = turned.reshape(channels, freq_rows, 2, width)
    result = jnp.einsum("asf,cfsb->cab", last_table, turned, precision=highest)
    return result / span_len


def body(
    gate_in,
    mult_in,
    value_in,
    taps_gate,
    taps_mult,
    taps_value,
    filter_first,
    filter_second,
    filter_ahead,
    filter_behind,
    filter_decay,
    skip_gain,
    out_weight,
):
    col_count = lax.axis_size("col")
    col_index = lax.axis_index("col")
    tok_rows = gate_in.shape[1]
    seq_len = tok_rows * col_count
    span_len = 2 * seq_len
    group_size = filter_ahead.shape[1] // col_count
    stacked = jnp.stack([gate_in[0], mult_in[0], value_in[0]])
    padded = padded_2(stacked, (("col", 1),), 1).astype(jnp.float32)
    all_taps = jnp.stack([taps_gate, taps_mult, taps_value])
    shorted = jnp.zeros(stacked.shape, jnp.float32)
    for offset in range(all_taps.shape[1]):
        shorted = shorted + all_taps[:, offset][:, None, :] * padded[:, offset : offset + tok_rows]
    gate_part = shorted[0]
    product = shorted[2] * shorted[1]
    spread = lax.all_to_all(product.T, "col", split_axis=0, concat_axis=1, tiled=True)
    first_channel = col_index * group_size
    own_rates = lax.dynamic_slice_in_dim(filter_decay, first_channel, group_size)
    mirror = lax.iota(jnp.int32, seq_len)
    hidden, tau_values = filter_hidden(mirror, seq_len, filter_first, filter_second)
    ahead_vals = side_values(
        hidden,
        tau_values,
        lax.dynamic_slice_in_dim(filter_ahead, first_channel, group_size, 1),
        own_rates,
    )
    behind_vals = side_values(
        hidden,
        tau_values,
        lax.dynamic_slice_in_dim(filter_behind, first_channel, group_size, 1),
        own_rates,
    )
    kernel = jnp.concatenate(
        [ahead_vals, jnp.zeros((group_size, 1), jnp.float32), jnp.flip(behind_vals[:, 1:], axis=1)],
        axis=1,
    )
    kernel = kernel * lax.rsqrt(jnp.sum(kernel * kernel, axis=1, keepdims=True) + 1e-06)
    factor = 128
    half_rows = factor // 2
    width_second = span_len // factor
    first_cos, first_sin = angle_table(factor, factor, factor)
    twist_cos, twist_sin = angle_table(factor, width_second, span_len)
    second_cos, second_sin = angle_table(width_second, width_second, width_second)
    first_table = jnp.stack([first_cos, -first_sin])
    last_table = jnp.stack([first_cos[:half_rows], -first_sin[:half_rows]], axis=1)
    twist_even = jnp.concatenate([twist_cos, twist_cos], axis=1)
    twist_ahead = jnp.concatenate([twist_sin, -twist_sin], axis=1)
    twist_back = jnp.concatenate([-twist_sin, twist_sin], axis=1)
    block_ahead = jnp.concatenate(
        [
            jnp.concatenate([second_cos, -second_sin], axis=1),
            jnp.concatenate([second_sin, second_cos], axis=1),
        ],
        axis=0,
    )
    block_back = jnp.concatenate(
        [
            jnp.concatenate([second_cos, second_sin], axis=1),
            jnp.concatenate([-second_sin, second_cos], axis=1),
        ],
        axis=0,
    )
    kernel_spec = forward(
        kernel.reshape(group_size, factor, width_second),
        first_table,
        twist_even,
        twist_ahead,
        block_ahead,
    )
    data_spec = forward(
        spread.reshape(group_size, half_rows, width_second),
        first_table[:, :, :half_rows],
        twist_even,
        twist_ahead,
        block_ahead,
    )
    data_re = data_spec[..., :width_second]
    data_im = data_spec[..., width_second:]
    kernel_re = kernel_spec[..., :width_second]
    kernel_im = kernel_spec[..., width_second:]
    joined = jnp.concatenate(
        [data_re * kernel_re - data_im * kernel_im, data_re * kernel_im + data_im * kernel_re],
        axis=-1,
    )
    convolved = inverse(joined, last_table, twist_even, twist_back, block_back, span_len).reshape(
        group_size, seq_len
    )
    returned = lax.all_to_all(convolved, "col", split_axis=1, concat_axis=0, tiled=True)
    mixed_rows = ((returned.T + skip_gain * product) * gate_part).astype(jnp.bfloat16)
    return jnp.dot(mixed_rows, out_weight, preferred_element_type=jnp.float32).astype(jnp.bfloat16)[
        None
    ]


def solution(mesh):
    in_specs = (
        P(("grp", "row"), "col", None),
        P(("grp", "row"), "col", None),
        P(("grp", "row"), "col", None),
        P(),
        P(),
        P(),
        P(),
        P(),
        P(),
        P(),
        P(),
        P(),
        P(),
    )
    out_specs = P(("grp", "row"), "col", None)
    return jax.shard_map(body, mesh=mesh, in_specs=in_specs, out_specs=out_specs, check_vma=False)
```

profile of v0, /device:TPU:0, one launch (start us, length us, event | category | flops | bytes accessed | tf_op | source)
XLA Modules:
  0.0 80.0 jit_solution(17331171744776615139)
XLA Ops:
  0.0 1.2 %copy.37 = bf16[1,128,1024]{1,2,0:T(8,128)(2,1)S(1)} copy(bf16[1,128,1024]{2,1,0:T(8,128)(2,1)} %param.13) | data formatting | bytes 524288 | tf_op args[0]
  1.2 1.2 %copy.38 = bf16[1,128,1024]{1,2,0:T(8,128)(2,1)S(1)} copy(bf16[1,128,1024]{2,1,0:T(8,128)(2,1)} %param.14) | data formatting | bytes 524288 | tf_op args[1]
  2.4 1.2 %copy.39 = bf16[1,128,1024]{1,2,0:T(8,128)(2,1)S(1)} copy(bf16[1,128,1024]{2,1,0:T(8,128)(2,1)} %param.15) | data formatting | bytes 524288 | tf_op args[2]
  3.7 0.7 copy-done.6
  4.4 0.1 pad_maximum_fusion.1
  4.5 0.0 copy-start.16
  4.5 0.3 fusion.116
  4.8 0.4 copy.40
  5.2 3.0 %collective-permute-start = (bf16[3,1,1024]{2,0,1:T(4,128)(2,1)S(1)}, bf16[3,1,1024]{2,0,1:T(4,128)(2,1)}, u32[]{:S(2)}, u32[]{:S(2)}) collective-permute-start(bf16[3,1,1024]{2,0,1:T(4,128)(2,1)S(1)} %copy.40), channel_id=1, source_target_pairs={{0,1},{1,2},{2,3},{4,5},{5,6},{6,7},{8,9},{9,10},{10,11},{12,13},{... | collective-permute-start | bytes 18440 | tf_op jit(solution)/shard_map/ppermute | solution.py:17
  8.1 1.0 %copy.41 = bf16[3,1,1024]{2,0,1:T(4,128)(2,1)} copy(bf16[3,1,1024]{1,2,0:T(8,128)(2,1)S(1)} %get-tuple-element.16) | data formatting | bytes 12288 | tf_op jit(solution)/shard_map/slice | solution.py:16
  9.1 1.3 %collective-permute-start.1 = (bf16[3,1,1024]{2,0,1:T(4,128)(2,1)}, bf16[3,1,1024]{2,0,1:T(4,128)(2,1)}, u32[]{:S(2)}, u32[]{:S(2)}) collective-permute-start(bf16[3,1,1024]{2,0,1:T(4,128)(2,1)} %copy.41), channel_id=1, source_target_pairs={{1,0},{2,1},{3,2},{5,4},{6,5},{7,6},{9,8},{10,9},{11,10},{13,12},{... | collective-permute-start | bytes 18440 | tf_op jit(solution)/shard_map/ppermute | solution.py:18
  10.5 0.3 sine_negate_fusion
  10.7 0.1 fusion.98
  10.8 0.7 fusion.96
  11.5 0.1 fusion.99
  11.6 0.1 pad_maximum_fusion.15
  11.6 0.2 multiply_cosine_fusion
  11.8 1.3 %convolution_sine_fusion.1 = f32[512,128]{1,0:T(8,128)S(1)} fusion(f32[33,128]{1,0:T(8,128)S(1)} %copy-done.16, f32[512,16]{0,1:T(8,128)S(1)} %get-tuple-element.25, f32[512,16]{0,1:T(8,128)S(1)} %get-tuple-element.24, f32[512,1]{0,1:T(1,128)S(1)} %convert_multiply_fusion.2), kind=kOutput, calls=%fused_computation.40 | convolution fusion | flops 25986048 | bytes 346624 | tf_op jit(solution)/shard_map/dot_general | solution.py:30
  13.2 1.2 %convolution_sine_fusion = f32[512,128]{1,0:T(8,128)S(1)} fusion(f32[512,128]{1,0:T(8,128)S(1)} %convolution_sine_fusion.1, f32[128,128]{1,0:T(8,128)S(1)} %copy-done.12), kind=kOutput, calls=%fused_computation.39 | convolution fusion | flops 100663296 | bytes 589824 | tf_op jit(solution)/shard_map/dot_general | solution.py:31
  14.4 0.8 dynamic-slice_negate_fusion
  15.1 0.6 fusion.48
  15.8 0.1 multiply_exponential_fusion
  15.9 0.3 slice_multiply_fusion.3
  16.3 0.8 reverse
  17.0 0.2 slice.164
  17.2 1.6 %convolution_multiply_fusion = f32[256,512]{1,0:T(8,128)S(1)} fusion(f32[512,128]{1,0:T(8,128)S(1)} %convolution_sine_fusion, f32[512]{0:T(512)S(1)} %convert_multiply_fusion, f32[256]{0:T(256)S(1)} %dynamic-slice_negate_fusion, f32[128,1024]{1,0:T(8,128)} %param.21, s32[]{:T(128)S(6)} %select_n.68), kind=kOutput, calls=%fused_computation.38 | convolution fusion | flops 201588736 | bytes 920580 | tf_op jit(solution)/shard_map/pf,fh->hp/dot_general | solution.py:36
  18.8 0.3 multiply_reduce_fusion
  19.1 0.3 copy.47
  19.5 0.1 fusion.36
  19.5 1.8 %convolution_bitcast_fusion = f32[256,128,2,8]{1,0,2,3:T(8,128)S(1)} fusion(f32[256,128,8,1]{0,2,1,3:T(8,128)S(1)} %fusion.36, f32[1,128,128]{1,2,0:T(8,128)S(1)} %get-tuple-element.28, f32[1,128,128]{1,2,0:T(8,128)S(1)} %get-tuple-element.29), kind=kOutput, calls=%fused_computation.27 | convolution fusion | flops 805339136 | bytes 3276800 | tf_op jit(solution)/shard_map/sfa,cab->cfsb/dot_general | solution.py:56
  21.4 1.2 %copy.80 = f32[256,128,2,8]{1,3,2,0:T(8,128)S(1)} copy(f32[256,128,2,8]{1,0,2,3:T(8,128)S(1)} %convolution_bitcast_fusion) | data formatting | bytes 4194304 | tf_op jit(solution)/shard_map/sfa,cab->cfsb/transpose | solution.py:56
  22.6 0.0 copy-start.18
  22.7 0.0 copy-start.19
  22.7 1.5 %fusion.115 = (f32[256,128,8]{1,2,0:T(8,128)}, f32[256,128,8]{1,2,0:T(8,128)}) fusion(f32[256,128,16]{1,2,0:T(8,128)S(1)} %bitcast.107), kind=kLoop, calls=%fused_computation.171 | loop fusion | bytes 4194304 | tf_op jit(solution)/shard_map/slice | solution.py:51
  24.1 0.8 cosine_bitcast_fusion
  24.9 0.6 pad_maximum_fusion.14
  25.5 0.6 copy_bitcast_fusion.2
  26.2 0.6 copy.82
  26.8 1.1 %copy.42 = bf16[3,1,1024]{1,2,0:T(8,128)(2,1)S(1)} copy(bf16[3,1,1024]{2,0,1:T(4,128)(2,1)} %collective-permute-done) | data formatting | bytes 12288 | tf_op jit(solution)/shard_map/ppermute | solution.py:17
  27.9 1.9 %copy.43 = bf16[3,1,1024]{1,2,0:T(8,128)(2,1)} copy(bf16[3,1,1024]{2,0,1:T(4,128)(2,1)} %collective-permute-done.1) | data formatting | bytes 12288 | tf_op jit(solution)/shard_map/ppermute | solution.py:18
  29.8 2.2 %maximum_convert_fusion = f32[3,130,1024]{1,2,0:T(8,128)S(1)} fusion(bf16[3,1,1024]{1,2,0:T(8,128)(2,1)} %copy.43, bf16[1,128,1024]{1,2,0:T(8,128)(2,1)} %copy-done.6, bf16[1,128,1024]{1,2,0:T(8,128)(2,1)} %copy-done.5, bf16[1,128,1024]{1,2,0:T(8,128)(2,1)} %copy-done.4, bf16[3,1,1024]{1,2,0:T(8,128)(2,1)S(1)} %copy.42), kind=kLoop, calls=%fused_computation.34 | loop fusion | flops 3993600 | bytes 2396160 | tf_op jit(solution)/shard_map/convert_element_type | solution.py:94
  32.1 2.3 %fusion.24 = f32[3,128,1024]{1,2,0:T(8,128)S(1)} fusion(f32[3,130,1024]{1,2,0:T(8,128)S(1)} %maximum_convert_fusion, f32[3,1024]{1,0:T(4,128)S(1)} %copy-done.9, f32[3,1024]{1,0:T(4,128)S(1)} %copy-done.10, f32[3,1024]{1,0:T(4,128)S(1)} %bitcast.114), kind=kLoop, calls=%fused_computation.30 | loop fusion | flops 1966080 | bytes 6328320 | tf_op jit(solution)/shard_map/add | solution.py:98
  34.4 1.1 %copy-done.1 = f32[3,128,1024]{1,2,0:T(8,128)} copy-done((f32[3,128,1024]{1,2,0:T(8,128)}, f32[3,128,1024]{1,2,0:T(8,128)S(1)}, u32[]{:S(2)}) %copy-start.1) | copy-done | bytes 1572888
  35.6 0.8 %slice_multiply_fusion.4 = f32[1,128,1024]{1,2,0:T(8,128)} fusion(f32[3,128,1024]{1,2,0:T(8,128)S(1)} %fusion.24), kind=kLoop, calls=%fused_computation.59 | loop fusion | flops 131072 | bytes 1572864 | tf_op jit(solution)/shard_map/mul | solution.py:100
  36.4 5.6 %all-to-all-start = ((f32[4,256,128]{2,1,0:T(8,128)}), f32[4,256,128]{2,1,0:T(8,128)S(1)}, u32[]{:S(2)}, u32[]{:S(2)}) async-start(f32[4,256,128]{2,1,0:T(8,128)} %bitcast.5), calls=%async_computation | async-start | bytes 1048576 | tf_op jit(solution)/shard_map/all_to_all | solution.py:101
  42.0 0.1 fusion.101
  42.0 6.1 %fusion.7 = f32[256,128,16]{1,2,0:T(8,128)} fusion(f32[256,128,8]{1,2,0:T(8,128)} %get-tuple-element.14, f32[256,128,8]{1,2,0:T(8,128)} %get-tuple-element.13, f32[128,16]{0,1:T(8,128)S(1)} %get-tuple-element.23, f32[128,16]{0,1:T(8,128)S(1)} %pad_maximum_fusion.12, f32[8,8]{0,1:T(8,128)S(1)} %copy-done.14, f32[8,8]{0,1:T(8,128)S(1)} %copy-done.13, ...), kind=kOutput, calls=%fused_computation.9 | convolution fusion | flops 102761216 | bytes 6308608 | tf_op jit(solution)/shard_map/cfk,kl->cfl/dot_general | solution.py:59
  48.1 2.7 %all-to-all-done = f32[4,256,128]{2,1,0:T(8,128)S(1)} async-done(((f32[4,256,128]{2,1,0:T(8,128)}), f32[4,256,128]{2,1,0:T(8,128)S(1)}, u32[]{:S(2)}, u32[]{:S(2)}) %all-to-all-start) | async-done | bytes 524320 | tf_op jit(solution)/shard_map/all_to_all | solution.py:101
  50.8 0.2 copy.44
  51.0 1.9 %convolution_bitcast_fusion.1 = f32[256,128,2,8]{1,0,2,3:T(8,128)S(1)} fusion(f32[256,64,8,1]{0,2,1,3:T(8,128)S(1)} %bitcast.113, f32[1,128,128]{1,2,0:T(8,128)S(1)} %get-tuple-element.29, f32[1,128,128]{1,2,0:T(8,128)S(1)} %get-tuple-element.28), kind=kOutput, calls=%fused_computation.28 | convolution fusion | flops 402669568 | bytes 2752512 | tf_op jit(solution)/shard_map/sfa,cab->cfsb/dot_general | solution.py:56
  52.9 1.2 %copy.81 = f32[256,128,2,8]{1,3,2,0:T(8,128)S(1)} copy(f32[256,128,2,8]{1,0,2,3:T(8,128)S(1)} %convolution_bitcast_fusion.1) | data formatting | bytes 4194304 | tf_op jit(solution)/shard_map/sfa,cab->cfsb/transpose | solution.py:56
  54.1 0.1 fusion.114
  54.2 3.1 %fusion.2 = f32[256,128,16]{1,2,0:T(8,128)S(1)} fusion(f32[256,128,8]{1,2,0:T(8,128)S(1)} %get-tuple-element.12, f32[256,128,8]{1,2,0:T(8,128)S(1)} %get-tuple-element.11, f32[128,16]{0,1:T(8,128)S(1)} %get-tuple-element.23, f32[128,16]{0,1:T(8,128)S(1)} %pad_maximum_fusion.12, f32[8,8]{0,1:T(8,128)S(1)} %copy-done.14, f32[8,8]{0,1:T(8,128)S(1)} %copy-done.13, ...), kind=kOutput, calls=%fused_computation.4 | convolution fusion | flops 102761216 | bytes 6308608 | tf_op jit(solution)/shard_map/cfk,kl->cfl/dot_general | solution.py:59
  57.4 0.2 multiply_subtract_fusion
  57.6 2.1 %fusion.11 = f32[256,128,16]{1,2,0:T(8,128)S(1)} fusion(f32[256,128,8]{1,2,0:T(8,128)S(1)} %get-tuple-element.8, f32[256,128,8]{1,2,0:T(8,128)S(1)} %get-tuple-element.7, f32[8,8]{0,1:T(8,128)S(1)} %copy-done.14, f32[8,8]{0,1:T(8,128)S(1)} %fusion.101, f32[8,8]{0,1:T(8,128)S(1)} %copy-done.13), kind=kOutput, calls=%fused_computation.12 | convolution fusion | flops 101188352 | bytes 4195072 | tf_op jit(solution)/shard_map/cfk,kl->cfl/dot_general | solution.py:65
  59.8 0.1 fusion.113
  59.9 0.6 copy-done.7
  60.5 0.0 copy-done.8
  60.5 1.8 %fusion.32 = f32[256,64,8]{1,2,0:T(8,128)S(1)} fusion(f32[256,128,8]{1,2,0:T(8,128)S(1)} %get-tuple-element.10, f32[256,128,8]{1,2,0:T(8,128)S(1)} %get-tuple-element.9, f32[256,128,16]{1,2,0:T(8,128)S(1)} %fusion.11, f32[128,16]{0,1:T(8,128)S(1)} %copy-done.15, f32[128,16]{0,1:T(8,128)S(1)} %pad_maximum_fusion.12, f32[64,1,128]{2,0,1:T(8,128)S(1)} %copy-done.8, ...), kind=kOutput, calls=%fused_computation.37 | convolution fusion | flops 404897792 | bytes 4800512 | tf_op jit(solution)/shard_map/asf,cfsb->cab/dot_general | solution.py:68
  62.4 1.2 %copy.51 = f32[256,64,8]{0,2,1:T(8,128)} copy(f32[256,64,8]{1,2,0:T(8,128)S(1)} %fusion.32) | data formatting | bytes 1048576 | tf_op jit(solution)/shard_map/div | solution.py:69
  63.6 12.3 %all_to_all.35 = f32[256,4,128]{0,2,1:T(8,128)S(1)} all-to-all(f32[256,4,128]{0,2,1:T(8,128)} %bitcast.110), channel_id=1, replica_groups=mesh['grp'=2,'row'=4,'col'=4] {'col'}, dimensions={1} | all-to-all | bytes 1048576 | tf_op jit(solution)/shard_map/all_to_all | solution.py:173
  75.8 0.2 copy.52
  76.1 0.2 fusion.44
  76.3 3.7 %fusion = bf16[1,128,2048]{2,1,0:T(8,128)(2,1)} fusion(bf16[128,1024]{0,1:T(8,128)(2,1)S(1)} %fusion.44, bf16[1024,2048]{1,0:T(8,128)(2,1)} %param.25), kind=kOutput, calls=%fused_computation.1 | convolution fusion | flops 537133056 | bytes 4980736 | tf_op jit(solution)/shard_map/dot_general | solution.py:175
  (46 shorter events, 0.2 us)
Async XLA Ops:
  0.0 15.1 %copy-start = (f32[128,1024]{1,0:T(8,128)S(1)}, f32[128,1024]{1,0:T(8,128)}, u32[]{:S(2)}) copy-start(f32[128,1024]{1,0:T(8,128)} %param.22) | copy-start | bytes 1572868
  1.2 2.5 %copy-start.4 = (bf16[1,128,1024]{1,2,0:T(8,128)(2,1)}, bf16[1,128,1024]{1,2,0:T(8,128)(2,1)S(1)}, u32[]{:S(2)}) copy-start(bf16[1,128,1024]{1,2,0:T(8,128)(2,1)S(1)} %copy.37) | copy-start | bytes 786436
  2.4 1.2 %copy-start.5 = (bf16[1,128,1024]{1,2,0:T(8,128)(2,1)}, bf16[1,128,1024]{1,2,0:T(8,128)(2,1)S(1)}, u32[]{:S(2)}) copy-start(bf16[1,128,1024]{1,2,0:T(8,128)(2,1)S(1)} %copy.38) | copy-start | bytes 786436
  3.7 0.7 copy-start.6
  4.5 7.4 %copy-start.16 = (f32[33,128]{1,0:T(8,128)S(1)}, f32[33,128]{1,0:T(8,128)}, u32[]{:S(2)}) copy-start(f32[33,128]{1,0:T(8,128)} %param.19) | copy-start | bytes 50692
  4.5 8.7 %copy-start.12 = (f32[128,128]{1,0:T(8,128)S(1)}, f32[128,128]{1,0:T(8,128)}, u32[]{:S(2)}) copy-start(f32[128,128]{1,0:T(8,128)} %param.20) | copy-start | bytes 196612
  5.2 21.6 %collective-permute-start = (bf16[3,1,1024]{2,0,1:T(4,128)(2,1)S(1)}, bf16[3,1,1024]{2,0,1:T(4,128)(2,1)}, u32[]{:S(2)}, u32[]{:S(2)}) collective-permute-start(bf16[3,1,1024]{2,0,1:T(4,128)(2,1)S(1)} %copy.40), channel_id=1, source_target_pairs={{0,1},{1,2},{2,3},{4,5},{5,6},{6,7},{8,9},{9,10},{10,11},{12,13},{... | collective-permute-start | bytes 18440 | tf_op jit(solution)/shard_map/ppermute | solution.py:17
  9.1 18.8 %collective-permute-start.1 = (bf16[3,1,1024]{2,0,1:T(4,128)(2,1)}, bf16[3,1,1024]{2,0,1:T(4,128)(2,1)}, u32[]{:S(2)}, u32[]{:S(2)}) collective-permute-start(bf16[3,1,1024]{2,0,1:T(4,128)(2,1)} %copy.41), channel_id=1, source_target_pairs={{1,0},{2,1},{3,2},{5,4},{6,5},{7,6},{9,8},{10,9},{11,10},{13,12},{... | collective-permute-start | bytes 18440 | tf_op jit(solution)/shard_map/ppermute | solution.py:18
  22.6 2.9 %copy-start.17 = (f32[3,1024]{1,0:T(4,128)S(1)}, f32[3,1024]{1,0:T(4,128)}, u32[]{:S(2)}) copy-start(f32[3,1024]{1,0:T(4,128)} %param.18) | copy-start | bytes 36868
  22.6 2.8 %copy-start.18 = (f32[3,1024]{1,0:T(4,128)S(1)}, f32[3,1024]{1,0:T(4,128)}, u32[]{:S(2)}) copy-start(f32[3,1024]{1,0:T(4,128)} %param.17) | copy-start | bytes 36868
  22.7 2.8 %copy-start.19 = (f32[3,1024]{1,0:T(4,128)S(1)}, f32[3,1024]{1,0:T(4,128)}, u32[]{:S(2)}) copy-start(f32[3,1024]{1,0:T(4,128)} %param.16) | copy-start | bytes 36868
  29.8 2.2 %copy-start.9 = (f32[3,1024]{1,0:T(4,128)S(1)}, f32[3,1024]{1,0:T(4,128)}, u32[]{:S(2)}) copy-start(f32[3,1024]{1,0:T(4,128)} %get-tuple-element.26) | copy-start | bytes 36868
  29.8 2.2 %copy-start.10 = (f32[3,1024]{1,0:T(4,128)S(1)}, f32[3,1024]{1,0:T(4,128)}, u32[]{:S(2)}) copy-start(f32[3,1024]{1,0:T(4,128)} %get-tuple-element.27) | copy-start | bytes 36868
  29.8 2.2 %copy-start.11 = (f32[3,1,1024]{2,0,1:T(4,128)S(1)}, f32[3,1,1024]{2,0,1:T(4,128)}, u32[]{:S(2)}) copy-start(f32[3,1,1024]{2,0,1:T(4,128)} %copy.82) | copy-start | bytes 36868
  34.4 1.1 %copy-start.1 = (f32[3,128,1024]{1,2,0:T(8,128)}, f32[3,128,1024]{1,2,0:T(8,128)S(1)}, u32[]{:S(2)}) copy-start(f32[3,128,1024]{1,2,0:T(8,128)S(1)} %fusion.24) | copy-start | bytes 4718596
  35.6 6.5 %copy-start.13 = (f32[8,8]{0,1:T(8,128)S(1)}, f32[8,8]{0,1:T(8,128)}, u32[]{:S(2)}) copy-start(f32[8,8]{0,1:T(8,128)} %get-tuple-element.32) | copy-start | bytes 772
  35.6 6.5 %copy-start.14 = (f32[8,8]{0,1:T(8,128)S(1)}, f32[8,8]{0,1:T(8,128)}, u32[]{:S(2)}) copy-start(f32[8,8]{0,1:T(8,128)} %get-tuple-element.33) | copy-start | bytes 772
  36.4 14.4 %all-to-all-start = ((f32[4,256,128]{2,1,0:T(8,128)}), f32[4,256,128]{2,1,0:T(8,128)S(1)}, u32[]{:S(2)}, u32[]{:S(2)}) async-start(f32[4,256,128]{2,1,0:T(8,128)} %bitcast.5), calls=%async_computation | async-start | bytes 1048576 | tf_op jit(solution)/shard_map/all_to_all | solution.py:101
  54.2 3.1 %copy-start.3 = (f32[256,128,16]{1,2,0:T(8,128)S(1)}, f32[256,128,16]{1,2,0:T(8,128)}, u32[]{:S(2)}) copy-start(f32[256,128,16]{1,2,0:T(8,128)} %fusion.7) | copy-start | bytes 6291460
  59.8 0.8 copy-start.7
  59.8 0.8 copy-start.8
  59.8 0.8 copy-start.15
  62.4 13.7 %copy-start.2 = (f32[3,128,1024]{1,2,0:T(8,128)S(1)}, f32[3,128,1024]{1,2,0:T(8,128)}, u32[]{:S(2)}) copy-start(f32[3,128,1024]{1,2,0:T(8,128)} %copy-done.1) | copy-start | bytes 4718596
  62.4 13.7 %copy-start.20 = (f32[1024]{0:T(1024)S(1)}, f32[1024]{0:T(1024)}, u32[]{:S(2)}) copy-start(f32[1024]{0:T(1024)} %param.24) | copy-start | bytes 12292
where the time goes:
time: 80.6 us; the launch traced here: 80 us
  matrix products  25.3 us (31%)
  local copies, waits for them, and re-layouts  19.1 us (24%)
  blocking collectives  12.3 us (15%)
  other arithmetic  10.3 us (13%)
  starting transfers between devices  9.83 us (12%)
  waiting for transfers between devices  2.68 us (3%)
    all_to_all x1, blocking collectives, body(): lax.all_to_all(convolved, 'col', split_axis=1, concat_axis=0, tiled=True)  12.3 us
    dot_general x2, matrix products, forward(): return jnp.einsum('cfk,kl->cfl', turned, second_block, precision=highest)  9.19 us
    unnamed x49, local copies, waits for them, and re-layouts  8.32 us
    all_to_all x1, starting transfers between devices, body(): lax.all_to_all(product.T, 'col', split_axis=0, concat_axis=1, tiled=True)  5.57 us
    dot_general x1, matrix products, body(): jnp.dot(mixed_rows, out_weight, preferred_element_type=jnp.float32)  3.73 us
    dot_general x2, matrix products, forward(): first = jnp.einsum('sfa,cab->cfsb', first_table, values, precision=highest)  3.72 us
    ppermute x1, starting transfers between devices, padded_2(): before = lax.ppermute(last, axis, up)  2.98 us
    all_to_all x1, waiting for transfers between devices, body(): lax.all_to_all(product.T, 'col', split_axis=0, concat_axis=1, tiled=True)  2.68 us
  transfers between devices with their start and end apart: 3, of which 1 were waited for; matrix products, arithmetic and copies ran while one was open for 30% of the time, Pallas kernels for 0%

commit v1 on v0

--- a/solution.py
+++ b/solution.py
@@ -98,7 +98,11 @@
         shorted = shorted + all_taps[:, offset][:, None, :] * padded[:, offset : offset + tok_rows]
     gate_part = shorted[0]
     product = shorted[2] * shorted[1]
-    spread = lax.all_to_all(product.T, "col", split_axis=0, concat_axis=1, tiled=True)
+    part = product.T
+    count = lax.axis_size("col")
+    tiles = jnp.stack(jnp.split(part, count, axis=0), axis=0)
+    tiles = lax.all_to_all(tiles, "col", split_axis=0, concat_axis=0)
+    spread = jnp.concatenate(tiles, axis=1)
     first_channel = col_index * group_size
     own_rates = lax.dynamic_slice_in_dim(filter_decay, first_channel, group_size)
     mirror = lax.iota(jnp.int32, seq_len)

time: 80.6 us -> 70.7 us (0.88)
  local copies, waits for them, and re-layouts: 19.1 us -> 11.4 us
  other arithmetic: 10.3 us -> 8.18 us
  blocking collectives: 12.3 us -> 11.2 us
  matrix products: 25.3 us -> 26.4 us
    unnamed x49 -> x36, local copies, waits for them, and re-layouts: 8.32 us -> 4.56 us
    ppermute x2 -> x0, local copies, waits for them, and re-layouts: 3.04 us -> none  [the longest x1 1.93 us: padded_2(): after = lax.ppermute(leading, axis, down)]
    add x1, other arithmetic: 2.33 us -> 0.46 us  [body(): shorted + all_taps[:, offset][:, None, :] * padded[:, offset:offset + tok...]
    convert_element_type x1, other arithmetic: 2.22 us -> 0.97 us  [body(): padded = padded_2(stacked, (('col', 1),), 1).astype(jnp.float32)]
    all_to_all x1, blocking collectives: 12.3 us -> 11.2 us  [body(): lax.all_to_all(convolved, 'col', split_axis=1, concat_axis=0, tiled=True)]
    another operation x0 -> x2, local copies, waits for them, and re-layouts: none -> 1.01 us  [the longest x1 0.97 us: body(): stacked = jnp.stack([gate_in[0], mult_in[0], value_in[0]])]
    slice x1 -> x0, local copies, waits for them, and re-layouts: 0.98 us -> none  [padded_2(): leading = lax.slice_in_dim(shard, 0, width, axis=dim)]
    mul x1 -> x0, other arithmetic: 0.85 us -> none  [body(): product = shorted[2] * shorted[1]]
  transfers between devices with their start and end apart: 3 -> 3, of which waited for: 1 -> 1; matrix products, arithmetic and copies ran while one was open for 30% -> 33% of each run, Pallas kernels for 0% -> 0%
where the time goes in v1:
time: 70.7 us; the launch traced here: 70.1 us
  matrix products  26.4 us (37%)
  local copies, waits for them, and re-layouts  11.4 us (16%)
  blocking collectives  11.2 us (16%)
  starting transfers between devices  9.83 us (14%)
  other arithmetic  8.18 us (12%)
  waiting for transfers between devices  2.68 us (4%)
    all_to_all x1, blocking collectives, body(): lax.all_to_all(convolved, 'col', split_axis=1, concat_axis=0, tiled=True)  11.2 us
    dot_general x2, matrix products, forward(): return jnp.einsum('cfk,kl->cfl', turned, second_block, precision=highest)  9.23 us
    all_to_all x1, starting transfers between devices, body(): tiles = lax.all_to_all(tiles, 'col', split_axis=0, concat_axis=0)  5.57 us
    unnamed x36, local copies, waits for them, and re-layouts  4.56 us
    dot_general x1, matrix products, body(): jnp.dot(mixed_rows, out_weight, preferred_element_type=jnp.float32)  4.3 us
    dot_general x2, matrix products, forward(): first = jnp.einsum('sfa,cab->cfsb', first_table, values, precision=highest)  3.72 us
    ppermute x1, starting transfers between devices, padded_2(): before = lax.ppermute(last, axis, up)  2.98 us
    all_to_all x1, waiting for transfers between devices, body(): tiles = lax.all_to_all(tiles, 'col', split_axis=0, concat_axis=0)  2.67 us
  transfers between devices with their start and end apart: 3, of which 1 were waited for; matrix products, arithmetic and copies ran while one was open for 33% of the time, Pallas kernels for 0%

profile of v1, /device:TPU:0, one launch (start us, length us, event | category | flops | bytes accessed | tf_op | source)
XLA Modules:
  0.0 70.1 jit_solution(16607664024362425979)
XLA Ops:
  0.0 0.0 copy-start
  0.0 1.0 %constant_dynamic-update-slice_fusion.2 = bf16[3,128,1024]{2,1,0:T(8,128)(2,1)S(1)} fusion(bf16[1,128,1024]{2,1,0:T(8,128)(2,1)} %param.13), kind=kLoop, calls=%fused_computation.129 | loop fusion | bytes 524288
  1.0 1.0 %constant_dynamic-update-slice_fusion.1 = bf16[3,128,1024]{2,1,0:T(8,128)(2,1)S(1)} fusion(bf16[3,128,1024]{2,1,0:T(8,128)(2,1)S(1)} %constant_dynamic-update-slice_fusion.2, bf16[1,128,1024]{2,1,0:T(8,128)(2,1)} %param.14), kind=kLoop, calls=%fused_computation.128 | loop fusion | bytes 524288
  2.0 1.0 %constant_dynamic-update-slice_fusion = bf16[3,128,1024]{2,1,0:T(8,128)(2,1)S(1)} fusion(bf16[3,128,1024]{2,1,0:T(8,128)(2,1)S(1)} %constant_dynamic-update-slice_fusion.1, bf16[1,128,1024]{2,1,0:T(8,128)(2,1)} %param.15), kind=kLoop, calls=%fused_computation.127 | loop fusion | bytes 524288 | tf_op jit(solution)/shard_map/stack | solution.py:93
  3.0 0.6 fusion.119
  3.6 3.0 %collective-permute-start = (bf16[3,1,1024]{2,1,0:T(2,128)(2,1)}, bf16[3,1,1024]{2,1,0:T(2,128)(2,1)}, u32[]{:S(2)}, u32[]{:S(2)}) collective-permute-start(bf16[3,1,1024]{2,1,0:T(2,128)(2,1)} %get-tuple-element.15), channel_id=1, source_target_pairs={{0,1},{1,2},{2,3},{4,5},{5,6},{6,7},{8,9},{9,10},{10,11},{12,13},{... | collective-permute-start | bytes 18440 | tf_op jit(solution)/shard_map/ppermute | solution.py:17
  6.6 1.3 %collective-permute-start.1 = (bf16[3,1,1024]{2,1,0:T(2,128)(2,1)}, bf16[3,1,1024]{2,1,0:T(2,128)(2,1)}, u32[]{:S(2)}, u32[]{:S(2)}) collective-permute-start(bf16[3,1,1024]{2,1,0:T(2,128)(2,1)} %get-tuple-element.16), channel_id=1, source_target_pairs={{1,0},{2,1},{3,2},{5,4},{6,5},{7,6},{9,8},{10,9},{11,10},{13,12},{... | collective-permute-start | bytes 18440 | tf_op jit(solution)/shard_map/ppermute | solution.py:18
  7.9 0.3 sine_negate_fusion
  8.2 0.1 fusion.101
  8.2 0.7 fusion.99
  8.9 0.6 fusion.102
  9.5 0.7 fusion.64
  10.2 0.1 pad_maximum_fusion.15
  10.3 0.2 multiply_cosine_fusion
  10.5 2.1 %convolution_sine_fusion.1 = f32[512,128]{1,0:T(8,128)S(1)} fusion(f32[33,128]{1,0:T(8,128)} %param.19, f32[512,16]{0,1:T(8,128)S(1)} %get-tuple-element.29, f32[512,16]{0,1:T(8,128)S(1)} %get-tuple-element.28, f32[512,1]{0,1:T(1,128)S(1)} %convert_multiply_fusion.2), kind=kOutput, calls=%fused_computation.39 | convolution fusion | flops 25986048 | bytes 346624 | tf_op jit(solution)/shard_map/dot_general | solution.py:30
  12.6 1.2 %convolution_sine_fusion = f32[512,128]{1,0:T(8,128)S(1)} fusion(f32[512,128]{1,0:T(8,128)S(1)} %convolution_sine_fusion.1, f32[128,128]{1,0:T(8,128)S(1)} %copy-done.6), kind=kOutput, calls=%fused_computation.38 | convolution fusion | flops 100663296 | bytes 589824 | tf_op jit(solution)/shard_map/dot_general | solution.py:31
  13.7 0.8 %dynamic-slice_negate_fusion = f32[256]{0:T(256)S(1)} fusion(f32[1024]{0:T(1024)} %param.23, s32[]{:T(128)S(6)} %select_n.68), kind=kLoop, calls=%fused_computation.163 | loop fusion | flops 256 | bytes 2052 | tf_op jit(solution)/shard_map/neg | solution.py:37
  14.5 0.6 fusion.51
  15.1 0.1 multiply_exponential_fusion
  15.3 0.3 slice_multiply_fusion.3
  15.6 0.8 %reverse = f32[256,512]{1,0:T(8,128)S(1)} reverse(f32[256,512]{1,0:T(8,128)S(1)} %bitcast.119), dimensions={1} | reverse | bytes 1048576
  16.4 0.2 slice.175
  16.6 1.6 %convolution_multiply_fusion = f32[256,512]{1,0:T(8,128)S(1)} fusion(f32[512,128]{1,0:T(8,128)S(1)} %convolution_sine_fusion, f32[512]{0:T(512)S(1)} %convert_multiply_fusion, f32[256]{0:T(256)S(1)} %dynamic-slice_negate_fusion, f32[128,1024]{1,0:T(8,128)} %param.21, s32[]{:T(128)S(6)} %select_n.68), kind=kOutput, calls=%fused_computation.37 | convolution fusion | flops 201588736 | bytes 920580 | tf_op jit(solution)/shard_map/pf,fh->hp/dot_general | solution.py:36
  18.2 0.3 multiply_reduce_fusion
  18.5 0.3 copy.28
  18.8 0.1 fusion.36
  18.9 1.8 %convolution_bitcast_fusion = f32[256,128,2,8]{1,0,2,3:T(8,128)S(1)} fusion(f32[256,128,8,1]{0,2,1,3:T(8,128)S(1)} %fusion.36, f32[1,128,128]{1,2,0:T(8,128)S(1)} %get-tuple-element.32, f32[1,128,128]{1,2,0:T(8,128)S(1)} %get-tuple-element.33), kind=kOutput, calls=%fused_computation.27 | convolution fusion | flops 805339136 | bytes 3276800 | tf_op jit(solution)/shard_map/sfa,cab->cfsb/dot_general | solution.py:56
  20.8 1.2 %copy.62 = f32[256,128,2,8]{1,3,2,0:T(8,128)S(1)} copy(f32[256,128,2,8]{1,0,2,3:T(8,128)S(1)} %convolution_bitcast_fusion) | data formatting | bytes 4194304 | tf_op jit(solution)/shard_map/sfa,cab->cfsb/transpose | solution.py:56
  22.0 0.0 copy-start.3
  22.0 0.0 copy-start.11
  22.0 0.0 copy-start.12
  22.0 0.0 copy-start.13
  22.0 1.5 %fusion.118 = (f32[256,128,8]{1,2,0:T(8,128)}, f32[256,128,8]{1,2,0:T(8,128)}) fusion(f32[256,128,16]{1,2,0:T(8,128)S(1)} %bitcast.117), kind=kLoop, calls=%fused_computation.180 | loop fusion | bytes 4194304 | tf_op jit(solution)/shard_map/slice | solution.py:51
  23.5 0.0 copy-done.3
  23.5 0.7 %cosine_bitcast_fusion = (f32[64,1,128]{2,0,1:T(8,128)}, f32[64,1,128]{2,0,1:T(8,128)}) fusion(f32[128,128]{1,0:T(8,128)S(1)} %copy-done.3), kind=kLoop, calls=%fused_computation.110 | loop fusion | flops 8192 | bytes 98304 | tf_op jit(solution)/shard_map/stack | solution.py:134
  24.3 0.0 copy-done.12
  24.3 0.6 pad_maximum_fusion.14
  24.9 0.0 collective-permute-done
  25.0 0.0 collective-permute-done.1
  25.0 1.0 %maximum_convert_fusion = f32[3,130,1024]{2,1,0:T(8,128)S(1)} fusion(bf16[3,1,1024]{2,1,0:T(2,128)(2,1)} %collective-permute-done.1, bf16[3,128,1024]{2,1,0:T(8,128)(2,1)S(1)} %constant_dynamic-update-slice_fusion, bf16[3,1,1024]{2,1,0:T(2,128)(2,1)} %collective-permute-done), kind=kLoop, calls=%fused_computation.53 | loop fusion | flops 2396160 | bytes 2396160 | tf_op jit(solution)/shard_map/convert_element_type | solution.py:94
  25.9 0.5 fusion.24
  26.4 1.1 %copy-done.2 = f32[3,128,1024]{2,1,0:T(8,128)} copy-done((f32[3,128,1024]{2,1,0:T(8,128)}, f32[3,128,1024]{2,1,0:T(8,128)S(1)}, u32[]{:S(2)}) %copy-start.2) | copy-done | bytes 1572888
  27.6 0.1 fusion.48
  27.7 0.8 %pad_maximum_fusion.1 = f32[4,256,128]{1,2,0:T(8,128)} fusion(f32[1,256,128]{1,2,0:T(8,128)S(1)} %get-tuple-element.18, f32[1,256,128]{1,2,0:T(8,128)S(1)} %get-tuple-element.19, f32[1,256,128]{1,2,0:T(8,128)S(1)} %get-tuple-element.20, f32[1,256,128]{1,2,0:T(8,128)S(1)} %get-tuple-element.17), kind=kLoop, calls=%fused_computation.59 | loop fusion | flops 393216 | bytes 1048576 | tf_op jit(solution)/shard_map/stack | solution.py:103
  28.5 5.6 %all-to-all-start = ((f32[4,256,128]{1,2,0:T(8,128)}), f32[4,256,128]{1,2,0:T(8,128)S(1)}, u32[]{:S(2)}, u32[]{:S(2)}) async-start(f32[4,256,128]{1,2,0:T(8,128)} %pad_maximum_fusion.1), calls=%async_computation | async-start | bytes 1048576 | tf_op jit(solution)/shard_map/all_to_all | solution.py:104
  34.1 0.1 fusion.100
  34.1 6.1 %fusion.7 = f32[256,128,16]{1,2,0:T(8,128)} fusion(f32[256,128,8]{1,2,0:T(8,128)} %get-tuple-element.14, f32[256,128,8]{1,2,0:T(8,128)} %get-tuple-element.13, f32[128,16]{0,1:T(8,128)S(1)} %get-tuple-element.27, f32[128,16]{0,1:T(8,128)S(1)} %pad_maximum_fusion.12, f32[8,8]{0,1:T(8,128)S(1)} %fusion.100, f32[8,8]{0,1:T(8,128)S(1)} %copy-done.7, ...), kind=kOutput, calls=%fused_computation.9 | convolution fusion | flops 102761216 | bytes 6308608 | tf_op jit(solution)/shard_map/cfk,kl->cfl/dot_general | solution.py:59
  40.2 2.7 %all-to-all-done = f32[4,256,128]{1,2,0:T(8,128)S(1)} async-done(((f32[4,256,128]{1,2,0:T(8,128)}), f32[4,256,128]{1,2,0:T(8,128)S(1)}, u32[]{:S(2)}, u32[]{:S(2)}) %all-to-all-start) | async-done | bytes 524320 | tf_op jit(solution)/shard_map/all_to_all | solution.py:104
  42.9 1.9 %convolution_bitcast_fusion.1 = f32[256,128,2,8]{1,0,2,3:T(8,128)S(1)} fusion(f32[256,64,8,1]{0,2,1,3:T(8,128)S(1)} %bitcast.123, f32[1,128,128]{1,2,0:T(8,128)S(1)} %get-tuple-element.33, f32[1,128,128]{1,2,0:T(8,128)S(1)} %get-tuple-element.32), kind=kOutput, calls=%fused_computation.28 | convolution fusion | flops 402669568 | bytes 2752512 | tf_op jit(solution)/shard_map/sfa,cab->cfsb/dot_general | solution.py:56
  44.8 1.2 %copy.63 = f32[256,128,2,8]{1,3,2,0:T(8,128)S(1)} copy(f32[256,128,2,8]{1,0,2,3:T(8,128)S(1)} %convolution_bitcast_fusion.1) | data formatting | bytes 4194304 | tf_op jit(solution)/shard_map/sfa,cab->cfsb/transpose | solution.py:56
  46.0 0.1 fusion.117
  46.1 3.2 %fusion.2 = f32[256,128,16]{1,2,0:T(8,128)S(1)} fusion(f32[256,128,8]{1,2,0:T(8,128)S(1)} %get-tuple-element.12, f32[256,128,8]{1,2,0:T(8,128)S(1)} %get-tuple-element.11, f32[128,16]{0,1:T(8,128)S(1)} %get-tuple-element.27, f32[128,16]{0,1:T(8,128)S(1)} %pad_maximum_fusion.12, f32[8,8]{0,1:T(8,128)S(1)} %fusion.100, f32[8,8]{0,1:T(8,128)S(1)} %copy-done.7, ...), kind=kOutput, calls=%fused_computation.4 | convolution fusion | flops 102761216 | bytes 6308608 | tf_op jit(solution)/shard_map/cfk,kl->cfl/dot_general | solution.py:59
  49.3 0.2 multiply_subtract_fusion
  49.6 1.9 %fusion.11 = f32[256,128,16]{1,2,0:T(8,128)S(1)} fusion(f32[256,128,8]{1,2,0:T(8,128)S(1)} %get-tuple-element.8, f32[256,128,8]{1,2,0:T(8,128)S(1)} %get-tuple-element.7, f32[8,8]{0,1:T(8,128)S(1)} %fusion.100, f32[8,8]{0,1:T(8,128)S(1)} %copy-done.8, f32[8,8]{0,1:T(8,128)S(1)} %copy-done.7), kind=kOutput, calls=%fused_computation.12 | convolution fusion | flops 101188352 | bytes 4195072 | tf_op jit(solution)/shard_map/cfk,kl->cfl/dot_general | solution.py:65
  51.5 0.0 copy-start.4
  51.5 0.0 copy-start.5
  51.5 0.4 fusion.116
  51.9 0.4 copy-done.4
  52.2 0.0 copy-done.5
  52.3 1.8 %fusion.32 = f32[256,64,8]{1,2,0:T(8,128)S(1)} fusion(f32[256,128,8]{1,2,0:T(8,128)S(1)} %get-tuple-element.10, f32[256,128,8]{1,2,0:T(8,128)S(1)} %get-tuple-element.9, f32[256,128,16]{1,2,0:T(8,128)S(1)} %fusion.11, f32[128,16]{0,1:T(8,128)S(1)} %copy-done.9, f32[128,16]{0,1:T(8,128)S(1)} %pad_maximum_fusion.12, f32[64,1,128]{2,0,1:T(8,128)S(1)} %copy-done.5, ...), kind=kOutput, calls=%fused_computation.36 | convolution fusion | flops 404897792 | bytes 4800512 | tf_op jit(solution)/shard_map/asf,cfsb->cab/dot_general | solution.py:68
  54.1 0.0 copy-start.14
  54.1 0.4 copy.32
  54.5 11.2 %all_to_all.24 = f32[256,4,128]{0,2,1:T(8,128)S(1)} all-to-all(f32[256,4,128]{0,2,1:T(8,128)S(1)} %bitcast.121), channel_id=1, replica_groups=mesh['grp'=2,'row'=4,'col'=4] {'col'}, dimensions={1} | all-to-all | bytes 1048576 | tf_op jit(solution)/shard_map/all_to_all | solution.py:177
  65.8 4.3 %fusion = bf16[1,128,2048]{2,1,0:T(8,128)(2,1)} fusion(bf16[1024,2048]{1,0:T(8,128)(2,1)} %param.25, f32[3,128,1024]{2,1,0:T(8,128)} %copy-done.2, f32[1024,128]{0,1:T(8,128)S(1)} %bitcast.120, f32[1024]{0:T(1024)S(1)} %copy-done.14), kind=kOutput, calls=%fused_computation.1 | convolution fusion | flops 537788416 | bytes 6819840 | tf_op jit(solution)/shard_map/dot_general | solution.py:179
  (29 shorter events, 0.2 us)
Async XLA Ops:
  0.0 14.5 %copy-start = (f32[128,1024]{1,0:T(8,128)S(1)}, f32[128,1024]{1,0:T(8,128)}, u32[]{:S(2)}) copy-start(f32[128,1024]{1,0:T(8,128)} %param.22) | copy-start | bytes 1572868
  0.0 12.6 %copy-start.6 = (f32[128,128]{1,0:T(8,128)S(1)}, f32[128,128]{1,0:T(8,128)}, u32[]{:S(2)}) copy-start(f32[128,128]{1,0:T(8,128)} %param.20) | copy-start | bytes 196612
  3.6 21.3 %collective-permute-start = (bf16[3,1,1024]{2,1,0:T(2,128)(2,1)}, bf16[3,1,1024]{2,1,0:T(2,128)(2,1)}, u32[]{:S(2)}, u32[]{:S(2)}) collective-permute-start(bf16[3,1,1024]{2,1,0:T(2,128)(2,1)} %get-tuple-element.15), channel_id=1, source_target_pairs={{0,1},{1,2},{2,3},{4,5},{5,6},{6,7},{8,9},{9,10},{10,11},{12,13},{... | collective-permute-start | bytes 18440 | tf_op jit(solution)/shard_map/ppermute | solution.py:17
  6.6 18.4 %collective-permute-start.1 = (bf16[3,1,1024]{2,1,0:T(2,128)(2,1)}, bf16[3,1,1024]{2,1,0:T(2,128)(2,1)}, u32[]{:S(2)}, u32[]{:S(2)}) collective-permute-start(bf16[3,1,1024]{2,1,0:T(2,128)(2,1)} %get-tuple-element.16), channel_id=1, source_target_pairs={{1,0},{2,1},{3,2},{5,4},{6,5},{7,6},{9,8},{10,9},{11,10},{13,12},{... | collective-permute-start | bytes 18440 | tf_op jit(solution)/shard_map/ppermute | solution.py:18
  22.0 1.5 %copy-start.3 = (f32[128,128]{1,0:T(8,128)S(1)}, f32[128,128]{1,0:T(8,128)}, u32[]{:S(2)}) copy-start(f32[128,128]{1,0:T(8,128)} %fusion.64) | copy-start | bytes 196612
  22.0 2.3 %copy-start.11 = (f32[3,1024]{1,0:T(4,128)S(1)}, f32[3,1024]{1,0:T(4,128)}, u32[]{:S(2)}) copy-start(f32[3,1024]{1,0:T(4,128)} %param.18) | copy-start | bytes 36868
  22.0 2.3 %copy-start.12 = (f32[3,1024]{1,0:T(4,128)S(1)}, f32[3,1024]{1,0:T(4,128)}, u32[]{:S(2)}) copy-start(f32[3,1024]{1,0:T(4,128)} %param.17) | copy-start | bytes 36868
  22.0 2.2 %copy-start.13 = (f32[3,1024]{1,0:T(4,128)S(1)}, f32[3,1024]{1,0:T(4,128)}, u32[]{:S(2)}) copy-start(f32[3,1024]{1,0:T(4,128)} %param.16) | copy-start | bytes 36868
  22.0 2.9 %copy-start.10 = (f32[128,8]{0,1:T(8,128)S(1)}, f32[128,8]{0,1:T(8,128)}, u32[]{:S(2)}) copy-start(f32[128,8]{0,1:T(8,128)} %fusion.102) | copy-start | bytes 12292
  26.4 1.1 %copy-start.2 = (f32[3,128,1024]{2,1,0:T(8,128)}, f32[3,128,1024]{2,1,0:T(8,128)S(1)}, u32[]{:S(2)}) copy-start(f32[3,128,1024]{2,1,0:T(8,128)S(1)} %fusion.24) | copy-start | bytes 4718596
  27.6 6.6 %copy-start.7 = (f32[8,8]{0,1:T(8,128)S(1)}, f32[8,8]{0,1:T(8,128)}, u32[]{:S(2)}) copy-start(f32[8,8]{0,1:T(8,128)} %get-tuple-element.36) | copy-start | bytes 772
  27.6 6.6 %copy-start.8 = (f32[8,8]{0,1:T(8,128)S(1)}, f32[8,8]{0,1:T(8,128)}, u32[]{:S(2)}) copy-start(f32[8,8]{0,1:T(8,128)} %get-tuple-element.37) | copy-start | bytes 772
  28.5 14.4 %all-to-all-start = ((f32[4,256,128]{1,2,0:T(8,128)}), f32[4,256,128]{1,2,0:T(8,128)S(1)}, u32[]{:S(2)}, u32[]{:S(2)}) async-start(f32[4,256,128]{1,2,0:T(8,128)} %pad_maximum_fusion.1), calls=%async_computation | async-start | bytes 1048576 | tf_op jit(solution)/shard_map/all_to_all | solution.py:104
  46.1 3.2 %copy-start.1 = (f32[256,128,16]{1,2,0:T(8,128)S(1)}, f32[256,128,16]{1,2,0:T(8,128)}, u32[]{:S(2)}) copy-start(f32[256,128,16]{1,2,0:T(8,128)} %fusion.7) | copy-start | bytes 6291460
  51.5 0.8 %copy-start.4 = (f32[64,1,128]{2,0,1:T(8,128)S(1)}, f32[64,1,128]{2,0,1:T(8,128)}, u32[]{:S(2)}) copy-start(f32[64,1,128]{2,0,1:T(8,128)} %get-tuple-element.21) | copy-start | bytes 98308
  51.5 0.8 %copy-start.5 = (f32[64,1,128]{2,0,1:T(8,128)S(1)}, f32[64,1,128]{2,0,1:T(8,128)}, u32[]{:S(2)}) copy-start(f32[64,1,128]{2,0,1:T(8,128)} %get-tuple-element.22) | copy-start | bytes 98308
  51.5 0.8 %copy-start.9 = (f32[128,16]{0,1:T(8,128)S(1)}, f32[128,16]{0,1:T(8,128)}, u32[]{:S(2)}) copy-start(f32[128,16]{0,1:T(8,128)} %get-tuple-element.26) | copy-start | bytes 24580
  54.1 11.7 %copy-start.14 = (f32[1024]{0:T(1024)S(1)}, f32[1024]{0:T(1024)}, u32[]{:S(2)}) copy-start(f32[1024]{0:T(1024)} %param.24) | copy-start | bytes 12292
